TPU v7x, 32 devices: a whole 2x2x4 slice. The times are simulated.
32 devices in a mesh: grp: 2 (over y), fs: 4 (over z), tp: 4 (over x, core).
Axes of the slice: x: 2, y: 2, z: 4, core: 2. Of those that a mesh axis runs over, the one named last changes fastest.
Arguments:
- stream_in: bfloat16 [3072, 2048], P(('grp', 'fs'), 'tp'), parts along dimension 0, may hold values from -6 to 6
- gain_before: bfloat16 [2048], P('tp'), may hold values from 0.099609375 to 1.8984375
- gain_mixer: bfloat16 [2048], P('tp'), may hold values from 0.099609375 to 1.8984375
- gain_after: bfloat16 [2048], P('tp'), may hold values from 0.099609375 to 1.8984375
- w_gate: bfloat16 [2048, 5632], P('fs', 'tp'), may hold values from -0.125 to 0.125
- w_upward: bfloat16 [2048, 5632], P('fs', 'tp'), may hold values from -0.125 to 0.125
- w_down: bfloat16 [5632, 2048], P('tp', 'fs'), may hold values from -0.078125 to 0.078125
- w_value: bfloat16 [2048, 1024], P('fs', 'tp'), may hold values from -0.125 to 0.125
- w_glu_gate: bfloat16 [2048, 1024], P('fs', 'tp'), may hold values from -0.125 to 0.125
- conv_taps: bfloat16 [31, 1024], P(None, 'tp'), may hold values from -1 to 1
- chan_gain: bfloat16 [1024], P('tp'), may hold values from 0.099609375 to 1.8984375
- chan_bias: bfloat16 [1024], P('tp'), may hold values from -3 to 3
- w_mix_out: bfloat16 [1024, 2048], P('tp', 'fs'), may hold values from -0.1875 to 0.1875
Outputs:
- stream_out: bfloat16 [3072, 2048], P(('grp', 'fs'), 'tp'), parts along dimension 0
There are 2 independent parts, one for each index of `grp`. A program takes and returns all parts, laid end to end along the dimension named above; an argument that names none is the same for every part. Nothing has to cross between parts.
All inputs are finite; a program needn't handle non-finite values.
Results may differ from a plain program's by a relative error of at most 0.017.
Values may be sent and summed in bfloat16 or wider, within the bound.
A program may use at most 64 MiB of HBM per device.

v0:
```python
import jax
import jax.numpy as jnp
from jax import lax
from jax.sharding import PartitionSpec as P

D = 2048
CHAN = 1024
KERNEL = 31
LEN = 128


epsilon = 1e-06


def normed_rows(stream, weights):
    values = stream.astype(jnp.float32)
    totals = lax.psum(jnp.sum(values * values, axis=1), "tp")
    inverse = lax.rsqrt(totals / D + epsilon)
    scaled = (values * inverse[:, None] * weights.astype(jnp.float32)).astype(jnp.bfloat16)
    return lax.all_gather(scaled, "tp", axis=1, tiled=True)


def settle(partial_term):
    return lax.psum_scatter(
        partial_term.astype(jnp.bfloat16), "tp", scatter_dimension=1, tiled=True
    ).astype(jnp.float32)


def pair_adder(rows, portions):
    return (
        jnp.dot(rows, portions[0], preferred_element_type=jnp.float32),
        jnp.dot(rows, portions[1], preferred_element_type=jnp.float32),
    )


def local(
    stream_in,
    gain_before,
    gain_mixer,
    gain_after,
    w_gate,
    w_upward,
    w_down,
    w_value,
    w_glu_gate,
    conv_taps,
    chan_gain,
    chan_bias,
    w_mix_out,
):
    whole_gate, whole_upward = (
        lax.all_gather(w_gate, "fs", axis=0, tiled=True),
        lax.all_gather(w_upward, "fs", axis=0, tiled=True),
    )
    whole_down = lax.all_gather(w_down, "fs", axis=1, tiled=True)

    def feed_forward(rows):
        gate = jnp.dot(rows, whole_gate, preferred_element_type=jnp.float32)
        upward = jnp.dot(rows, whole_upward, preferred_element_type=jnp.float32)
        hidden = (jax.nn.silu(gate) * upward).astype(jnp.bfloat16)
        return settle(jnp.dot(hidden, whole_down, preferred_element_type=jnp.float32))

    first = (
        stream_in.astype(jnp.float32) + 0.5 * feed_forward(normed_rows(stream_in, gain_before))
    ).astype(jnp.bfloat16)
    rows = normed_rows(first, gain_mixer)
    value, gating = pair_adder(
        rows,
        (
            lax.all_gather(w_value, "fs", axis=0, tiled=True),
            lax.all_gather(w_glu_gate, "fs", axis=0, tiled=True),
        ),
    )
    glued = value * jax.nn.sigmoid(gating)
    channels = glued.shape[1]
    grouped = glued.reshape(-1, LEN, channels)
    padded = jnp.pad(grouped, ((0, 0), (KERNEL - 1, 0), (0, 0)))
    taps = conv_taps.astype(jnp.float32)
    conv_sum = jnp.zeros_like(grouped)
    for lag_index in range(KERNEL):
        conv_sum = conv_sum + taps[lag_index] * padded[:, lag_index : lag_index + LEN]
    flat = conv_sum.reshape(-1, channels)
    sum_plain, sum_square = lax.psum((jnp.sum(flat, axis=1), jnp.sum(flat * flat, axis=1)), "tp")
    average = sum_plain / CHAN
    spread = sum_square / CHAN - average * average
    normed = (flat - average[:, None]) * lax.rsqrt(spread + epsilon)[:, None] * chan_gain.astype(
        jnp.float32
    ) + chan_bias.astype(jnp.float32)
    mixed = jax.nn.silu(normed).astype(jnp.bfloat16)
    branch = settle(
        jnp.dot(
            mixed,
            lax.all_gather(w_mix_out, "fs", axis=1, tiled=True),
            preferred_element_type=jnp.float32,
        )
    )
    second = (first.astype(jnp.float32) + branch).astype(jnp.bfloat16)
    third = second.astype(jnp.float32) + 0.5 * feed_forward(normed_rows(second, gain_after))
    return third.astype(jnp.bfloat16)


def solution(mesh):
    in_specs = (
        P(("grp", "fs"), "tp"),
        P("tp"),
        P("tp"),
        P("tp"),
        P("fs", "tp"),
        P("fs", "tp"),
        P("tp", "fs"),
        P("fs", "tp"),
        P("fs", "tp"),
        P(None, "tp"),
        P("tp"),
        P("tp"),
        P("tp", "fs"),
    )
    out_specs = P(("grp", "fs"), "tp")
    return jax.shard_map(local, mesh=mesh, in_specs=in_specs, out_specs=out_specs, check_vma=False)
```

profile of v0, /device:TPU:0, one launch (start us, length us, event | category | flops | bytes accessed | tf_op | source)
XLA Modules:
  0.0 621.5 jit_solution(9285012846678783133)
XLA Ops:
  6.5 1.2 fusion.5
  7.7 8.4 %psum.35 = f32[384]{0:T(512)S(1)} all-reduce(f32[384]{0:T(512)S(1)} %fusion.5), channel_id=1, replica_groups=mesh['grp'=2,'fs'=4,'tp'=4] {'tp'}, use_global_device_ids=true, to_apply=%region_1.0 | all-reduce | flops 384 | bytes 3072 | tf_op jit(solution)/shard_map/psum | solution.py:17
  16.1 0.7 convert_element_type.78
  16.8 1.9 fusion.7
  18.7 0.0 all-gather.12.cloned.1.call-start
  18.7 0.7 all-gather.12.cloned.1.call-update
  19.4 0.0 all-gather.14.cloned.1.call-start
  19.5 0.7 all-gather.14.cloned.1.call-update
  20.2 0.5 all-gather.16.cloned.1.call-update
  20.7 0.0 reduce-scatter.4.cloned.1.call-start
  20.8 18.0 %all-gather.10.cloned.1.call-done = bf16[384,2048]{1,0:T(8,128)(2,1)} async-done(((bf16[384,512]{1,0:T(8,128)(2,1)}), bf16[384,2048]{1,0:T(8,128)(2,1)}) %all-gather.10.cloned.1.call-update) | async-done | bytes 1572880 | tf_op jit(solution)/shard_map/all_gather | solution.py:20
  38.8 108.3 %all-gather.12.cloned.1.call-done = bf16[2048,1408]{1,0:T(8,128)(2,1)} async-done(((bf16[512,1408]{1,0:T(8,128)(2,1)}), bf16[2048,1408]{1,0:T(8,128)(2,1)}) %all-gather.12.cloned.1.call-update) | async-done | bytes 5767184 | tf_op jit(solution)/shard_map/all_gather | solution.py:52
  147.1 7.1 %fusion.87 = f32[384,1408]{1,0:T(8,128)} fusion(bf16[384,2048]{1,0:T(8,128)(2,1)} %all-gather.10.cloned.1.call-done, bf16[2048,1408]{1,0:T(8,128)(2,1)} %all-gather.12.cloned.1.call-done), kind=kOutput, calls=%fused_computation.139 | convolution fusion | flops 2214592512 | bytes 9502720 | tf_op jit(solution)/shard_map/dot_general | solution.py:58
  154.1 99.5 %all-gather.14.cloned.1.call-done = bf16[2048,1408]{1,0:T(8,128)(2,1)} async-done(((bf16[512,1408]{1,0:T(8,128)(2,1)}), bf16[2048,1408]{1,0:T(8,128)(2,1)}) %all-gather.14.cloned.1.call-update) | async-done | bytes 5767184 | tf_op jit(solution)/shard_map/all_gather | solution.py:53
  253.6 106.4 %all-gather.16.cloned.1.call-done = bf16[1408,2048]{1,0:T(8,128)(2,1)} async-done(((bf16[1408,512]{1,0:T(8,128)(2,1)}), bf16[1408,2048]{1,0:T(8,128)(2,1)}) %all-gather.16.cloned.1.call-update) | async-done | bytes 5767184 | tf_op jit(solution)/shard_map/all_gather | solution.py:55
  360.0 11.2 %convolution_convert_fusion.1 = bf16[384,2048]{1,0:T(8,128)(2,1)} fusion(bf16[1408,2048]{1,0:T(8,128)(2,1)} %all-gather.16.cloned.1.call-done, bf16[384,2048]{1,0:T(8,128)(2,1)S(1)} %copy-done.6, bf16[2048,1408]{1,0:T(8,128)(2,1)} %all-gather.14.cloned.1.call-done, f32[384,1408]{1,0:T(8,128)} %fusion.87), kind=kOutput, calls=%fused_computation.5 | convolution fusion | flops 4433215488 | bytes 16842752 | tf_op jit(solution)/shard_map/dot_general | solution.py:61
  371.3 0.0 all-gather.22.cloned.1.call-start
  371.3 0.5 all-gather.22.cloned.1.call-update
  371.8 0.0 all-gather.18.cloned.1.call-start
  371.9 25.8 %reduce-scatter.4.cloned.1.call-done = bf16[384,512]{1,0:T(8,128)(2,1)} async-done(((bf16[384,2048]{1,0:T(8,128)(2,1)}), bf16[384,512]{1,0:T(8,128)(2,1)}) %reduce-scatter.4.cloned.1.call-update) | async-done | bytes 393232 | tf_op jit(solution)/shard_map/reduce_scatter | solution.py:24
  397.7 1.2 fusion.9
  398.9 5.8 psum.36
  404.7 0.9 fusion.11
  405.6 0.0 all-gather.20.cloned.1.call-start
  405.7 0.7 all-gather.20.cloned.1.call-update
  406.4 0.7 all-gather.24.cloned.1.call-update
  407.1 0.0 reduce-scatter.6.cloned.1.call-start
  407.2 19.8 %all-gather.22.cloned.1.call-done = bf16[2048,256]{1,0:T(8,128)(2,1)} async-done(((bf16[512,256]{1,0:T(8,128)(2,1)}), bf16[2048,256]{1,0:T(8,128)(2,1)}) %all-gather.22.cloned.1.call-update) | async-done | bytes 1048592 | tf_op jit(solution)/shard_map/all_gather | solution.py:71
  427.1 20.6 %all-gather.18.cloned.1.call-done = bf16[384,2048]{1,0:T(8,128)(2,1)} async-done(((bf16[384,512]{1,0:T(8,128)(2,1)}), bf16[384,2048]{1,0:T(8,128)(2,1)}) %all-gather.18.cloned.1.call-update) | async-done | bytes 1572880 | tf_op jit(solution)/shard_map/all_gather | solution.py:20
  447.7 2.4 fusion.4
  450.1 27.2 %all-gather.20.cloned.1.call-done = bf16[2048,256]{1,0:T(8,128)(2,1)} async-done(((bf16[512,256]{1,0:T(8,128)(2,1)}), bf16[2048,256]{1,0:T(8,128)(2,1)}) %all-gather.20.cloned.1.call-update) | async-done | bytes 1048592 | tf_op jit(solution)/shard_map/all_gather | solution.py:70
  477.3 1.8 convolution_multiply_fusion.2
  479.1 1.6 fusion.82
  480.7 6.1 all-reduce.1
  486.7 0.2 multiply_convert_fusion
  487.0 19.3 %all-gather.24.cloned.1.call-done = bf16[256,2048]{1,0:T(8,128)(2,1)} async-done(((bf16[256,512]{1,0:T(8,128)(2,1)}), bf16[256,2048]{1,0:T(8,128)(2,1)}) %all-gather.24.cloned.1.call-update) | async-done | bytes 1048592 | tf_op jit(solution)/shard_map/all_gather | solution.py:93
  506.3 3.0 convolution_convert_fusion.2
  509.2 0.0 all-gather.26.cloned.1.call-start
  509.3 27.5 %reduce-scatter.6.cloned.1.call-done = bf16[384,512]{1,0:T(8,128)(2,1)} async-done(((bf16[384,2048]{1,0:T(8,128)(2,1)}), bf16[384,512]{1,0:T(8,128)(2,1)}) %reduce-scatter.6.cloned.1.call-update) | async-done | bytes 393232 | tf_op jit(solution)/shard_map/reduce_scatter | solution.py:24
  536.8 1.2 fusion.13
  538.0 5.8 psum.39
  543.7 1.9 fusion.15
  545.7 0.2 reduce-scatter.8.cloned.1.call-start
  545.9 20.2 %all-gather.26.cloned.1.call-done = bf16[384,2048]{1,0:T(8,128)(2,1)} async-done(((bf16[384,512]{1,0:T(8,128)(2,1)}), bf16[384,2048]{1,0:T(8,128)(2,1)}) %all-gather.26.cloned.1.call-update) | async-done | bytes 1572880 | tf_op jit(solution)/shard_map/all_gather | solution.py:20
  566.1 7.2 %fusion.88 = f32[384,1408]{1,0:T(8,128)} fusion(bf16[384,2048]{1,0:T(8,128)(2,1)} %all-gather.26.cloned.1.call-done, bf16[2048,1408]{1,0:T(8,128)(2,1)} %all-gather.12.cloned.1.call-done), kind=kOutput, calls=%fused_computation.140 | convolution fusion | flops 2214592512 | bytes 9502720 | tf_op jit(solution)/shard_map/dot_general | solution.py:58
  573.3 11.3 %convolution_convert_fusion = bf16[384,2048]{1,0:T(8,128)(2,1)} fusion(bf16[1408,2048]{1,0:T(8,128)(2,1)} %all-gather.16.cloned.1.call-done, bf16[384,2048]{1,0:T(8,128)(2,1)S(1)} %copy-done.7, bf16[2048,1408]{1,0:T(8,128)(2,1)} %all-gather.14.cloned.1.call-done, f32[384,1408]{1,0:T(8,128)} %fusion.88), kind=kOutput, calls=%fused_computation.4 | convolution fusion | flops 4433215488 | bytes 16842752 | tf_op jit(solution)/shard_map/dot_general | solution.py:61
  584.6 28.1 %reduce-scatter.8.cloned.1.call-done = bf16[384,512]{1,0:T(8,128)(2,1)} async-done(((bf16[384,2048]{1,0:T(8,128)(2,1)}), bf16[384,512]{1,0:T(8,128)(2,1)}) %reduce-scatter.8.cloned.1.call-update) | async-done | bytes 393232 | tf_op jit(solution)/shard_map/reduce_scatter | solution.py:24
  612.8 1.9 fusion.16
  (39 shorter events, 0.3 us)
Async XLA Ops:
  6.5 32.2 %all-gather.10.cloned.1.call-start = ((), (), s32[]{:S(2)}) async-start(), calls=%async_computation.3 | async-start | bytes 1966080 | tf_op jit(solution)/shard_map/all_gather | solution.py:20
  18.7 128.4 %all-gather.12.cloned.1.call-start = ((), (), s32[]{:S(2)}) async-start(), calls=%async_computation.4 | async-start | bytes 7208960 | tf_op jit(solution)/shard_map/all_gather | solution.py:52
  19.4 234.2 %all-gather.14.cloned.1.call-start = ((), (), s32[]{:S(2)}) async-start(), calls=%async_computation.5 | async-start | bytes 7208960 | tf_op jit(solution)/shard_map/all_gather | solution.py:53
  20.2 339.9 %all-gather.16.cloned.1.call-start = ((), (), s32[]{:S(2)}) async-start(), calls=%async_computation.6 | async-start | bytes 7208960 | tf_op jit(solution)/shard_map/all_gather | solution.py:55
  20.7 376.9 %reduce-scatter.4.cloned.1.call-start = ((), (), s32[]{:S(2)}) async-start(), calls=%async_computation.7 | async-start | bytes 1966080 | tf_op jit(solution)/shard_map/reduce_scatter | solution.py:24
  38.8 321.3 %copy-start.6 = (bf16[384,2048]{1,0:T(8,128)(2,1)S(1)}, bf16[384,2048]{1,0:T(8,128)(2,1)}, u32[]{:S(2)}) copy-start(bf16[384,2048]{1,0:T(8,128)(2,1)} %all-gather.10.cloned.1.call-done) | copy-start | bytes 4718596
  154.1 217.7 %copy-start.4 = (bf16[512]{0:T(512)(128)(2,1)S(1)}, bf16[512]{0:T(512)(128)(2,1)}, u32[]{:S(2)}) copy-start(bf16[512]{0:T(512)(128)(2,1)} %param.15) | copy-start | bytes 3076
  154.1 243.5 %copy-start = (bf16[384,512]{1,0:T(8,128)(2,1)S(1)}, bf16[384,512]{1,0:T(8,128)(2,1)}, u32[]{:S(2)}) copy-start(bf16[384,512]{1,0:T(8,128)(2,1)} %param.13) | copy-start | bytes 1179652
  371.2 35.9 %copy-start.3 = (bf16[31,256]{1,0:T(8,128)(2,1)S(1)}, bf16[31,256]{1,0:T(8,128)(2,1)}, u32[]{:S(2)}) copy-start(bf16[31,256]{1,0:T(8,128)(2,1)} %param.22) | copy-start | bytes 47620
  371.2 36.0 %copy-start.8 = (bf16[256]{0:T(256)(128)(2,1)S(1)}, bf16[256]{0:T(256)(128)(2,1)}, u32[]{:S(2)}) copy-start(bf16[256]{0:T(256)(128)(2,1)} %param.23) | copy-start | bytes 1540
  371.2 36.0 %copy-start.9 = (bf16[256]{0:T(256)(128)(2,1)S(1)}, bf16[256]{0:T(256)(128)(2,1)}, u32[]{:S(2)}) copy-start(bf16[256]{0:T(256)(128)(2,1)} %param.24) | copy-start | bytes 1540
  371.3 55.8 %all-gather.22.cloned.1.call-start = ((), (), s32[]{:S(2)}) async-start(), calls=%async_computation.10 | async-start | bytes 1310720 | tf_op jit(solution)/shard_map/all_gather | solution.py:71
  371.8 75.9 %all-gather.18.cloned.1.call-start = ((), (), s32[]{:S(2)}) async-start(), calls=%async_computation.8 | async-start | bytes 1966080 | tf_op jit(solution)/shard_map/all_gather | solution.py:20
  405.6 71.7 %all-gather.20.cloned.1.call-start = ((), (), s32[]{:S(2)}) async-start(), calls=%async_computation.9 | async-start | bytes 1310720 | tf_op jit(solution)/shard_map/all_gather | solution.py:70
  406.4 99.9 %all-gather.24.cloned.1.call-start = ((), (), s32[]{:S(2)}) async-start(), calls=%async_computation.11 | async-start | bytes 1310720 | tf_op jit(solution)/shard_map/all_gather | solution.py:93
  407.1 129.7 %reduce-scatter.6.cloned.1.call-start = ((), (), s32[]{:S(2)}) async-start(), calls=%async_computation.12 | async-start | bytes 1966080 | tf_op jit(solution)/shard_map/reduce_scatter | solution.py:24
  447.7 29.6 %copy-start.2 = (bf16[384,2048]{1,0:T(8,128)(2,1)S(1)}, bf16[384,2048]{1,0:T(8,128)(2,1)}, u32[]{:S(2)}) copy-start(bf16[384,2048]{1,0:T(8,128)(2,1)} %all-gather.18.cloned.1.call-done) | copy-start | bytes 4718596
  487.0 22.3 %copy-start.5 = (bf16[512]{0:T(512)(128)(2,1)S(1)}, bf16[512]{0:T(512)(128)(2,1)}, u32[]{:S(2)}) copy-start(bf16[512]{0:T(512)(128)(2,1)} %param.16) | copy-start | bytes 3076
  509.2 56.8 %all-gather.26.cloned.1.call-start = ((), (), s32[]{:S(2)}) async-start(), calls=%async_computation.13 | async-start | bytes 1966080 | tf_op jit(solution)/shard_map/all_gather | solution.py:20
  545.7 67.1 %reduce-scatter.8.cloned.1.call-start = ((), (), s32[]{:S(2)}) async-start(), calls=%async_computation.14 | async-start | bytes 1966080 | tf_op jit(solution)/shard_map/reduce_scatter | solution.py:24
  566.1 7.2 %copy-start.7 = (bf16[384,2048]{1,0:T(8,128)(2,1)S(1)}, bf16[384,2048]{1,0:T(8,128)(2,1)}, u32[]{:S(2)}) copy-start(bf16[384,2048]{1,0:T(8,128)(2,1)} %all-gather.26.cloned.1.call-done) | copy-start | bytes 4718596
  573.3 39.5 %copy-start.1 = (bf16[384,512]{1,0:T(8,128)(2,1)S(1)}, bf16[384,512]{1,0:T(8,128)(2,1)}, u32[]{:S(2)}) copy-start(bf16[384,512]{1,0:T(8,128)(2,1)} %reduce-scatter.6.cloned.1.call-done) | copy-start | bytes 1179652
Sparse Core Ops, SparseCore 0:
  18.8 19.9 all-gather.9
  40.4 106.6 all-gather.11
  148.7 104.9 all-gather.13
  255.1 104.9 all-gather.15
  371.4 26.2 reduce-scatter.3
  399.1 27.9 all-gather.21
  428.7 18.9 all-gather.17
  449.3 27.9 all-gather.19
  478.9 27.3 all-gather.23
  509.4 27.3 reduce-scatter.5
  545.8 20.2 all-gather.25
  584.7 27.9 reduce-scatter.7
where the time goes:
time: 622 us
  waiting for transfers between devices  525 us (84%)
  matrix products  43.9 us (7%)
  blocking collectives  26 us (4%)
  between operations  13.7 us (2%)
  other arithmetic  12.7 us (2%)
    all_gather x1, waiting for transfers between devices, local(): lax.all_gather(w_gate, 'fs', axis=0, tiled=True)  108 us
    all_gather x1, waiting for transfers between devices, local(): whole_down = lax.all_gather(w_down, 'fs', axis=1, tiled=True)  106 us
    all_gather x1, waiting for transfers between devices, local(): lax.all_gather(w_upward, 'fs', axis=0, tiled=True)  99.5 us
    reduce_scatter x3, waiting for transfers between devices, settle(): lax.psum_scatter(partial_term.astype(jnp.bfloat16), 'tp', scatter_dimensi...  81.4 us
    all_gather x3, waiting for transfers between devices, normed_rows(): return lax.all_gather(scaled, 'tp', axis=1, tiled=True)  58.8 us
    all_gather x1, waiting for transfers between devices, local(): lax.all_gather(w_value, 'fs', axis=0, tiled=True)  27.2 us
    dot_general x2, matrix products, feed_forward(): jnp.dot(hidden, whole_down, preferred_element_type=jnp.float32)  22.5 us
    psum x3, blocking collectives, normed_rows(): totals = lax.psum(jnp.sum(values * values, axis=1), 'tp')  19.9 us
  transfers between devices with their start and end apart: 12, of which 12 were waited for; matrix products, arithmetic and copies ran while one was open for 2% of the time, Pallas kernels for 0%

commit v1 on v0

v1 whole, which is shorter than its diff:
```python
import functools

import jax
import jax.numpy as jnp
from jax import lax
from jax.experimental import pallas as pl
from jax.experimental.pallas import tpu as pltpu
from jax.sharding import PartitionSpec as P

KERNEL = 31
LEN = 128
WIDE = 384
LEAD = 3
SUB = 16

epsilon = 1e-06
MESH = pl.DeviceIdType.MESH
f32 = jnp.float32
bf16 = jnp.bfloat16


def aligned(value, step):
    return pl.multiple_of(value, step)


def kernel(
    cfg,
    x_hbm,
    gate_hbm,
    up_hbm,
    down_hbm,
    value_hbm,
    glu_hbm,
    mix_hbm,
    gains_ref,
    small_ref,
    out_ref,
    *scratch,
):
    n_grp, n_fs, n_tp = cfg["n_grp"], cfg["n_fs"], cfg["n_tp"]
    R, E, DK, F, C, widths = cfg["R"], cfg["E"], cfg["DK"], cfg["F"], cfg["C"], cfg["widths"]
    D = E * n_tp
    n_x = n_tp // 2
    n_ch = R // LEN
    n_b = len(widths)
    scratch = list(scratch)
    take = lambda count: [scratch.pop(0) for _ in range(count)]
    gates, ups, downs = take(n_b), take(n_b), take(n_b)
    value_w, glu_w, mix_w = take(3)
    xfull, nbuf, acc, hbuf, pad_ref, conv_ref, gfull = take(7)
    rs1_s, rs1_r, rs2_s, rs2_r, st_s, st_r = take(6)
    sem_own, sem_x = take(2)
    recv_z, recv_y, send_r, send_l, send_y = take(5)
    ga_s, ga_r, ag_s, ag_r, s1_s, s1_r, s2_s, s2_r, ss_s, ss_r = take(10)

    g = lax.axis_index("grp")
    z = lax.axis_index("fs")
    tp = lax.axis_index("tp")
    xi = lax.div(tp, 2)
    par = lax.rem(tp, 2)
    partner = xi * 2 + 1 - par

    pieces = []
    start = 0
    for b, w in enumerate(widths):
        pieces.append((gates[b], gate_hbm.at[:, pl.ds(start, w)], "row"))
        pieces.append((ups[b], up_hbm.at[:, pl.ds(start, w)], "row"))
        pieces.append((downs[b], down_hbm.at[pl.ds(start, w), :], "col"))
        start += w
    pieces.append((value_w, value_hbm, "row"))
    pieces.append((glu_w, glu_hbm, "row"))
    pieces.append((mix_w, mix_hbm, "col"))
    n_p = len(pieces)

    def whole_of(p, src):
        ref, _, kind = pieces[p]
        if kind == "row":
            return ref.at[pl.ds(aligned(src * DK, DK), DK), :]
        return ref.at[src]

    def part_of(p, src, half):
        ref, _, kind = pieces[p]
        if kind == "row":
            size = DK // n_grp
            return ref.at[pl.ds(aligned(src * DK + half * size, size), size), :]
        size = ref.shape[1] // n_grp
        return ref.at[src, pl.ds(aligned(half * size, size), size), :]

    def own_copy(p):
        return pltpu.make_async_copy(pieces[p][1], whole_of(p, z), sem_own.at[p])

    def hop(p, src, sends, to):
        part = part_of(p, src, g)
        return pltpu.make_async_remote_copy(
            src_ref=part, dst_ref=part, send_sem=sends.at[p, src], recv_sem=recv_z.at[p, src],
            device_id={"fs": to}, device_id_type=MESH)

    def right(p, src):
        return hop(p, src, send_r, jnp.minimum(z + 1, n_fs - 1))

    def left(p, src):
        return hop(p, src, send_l, jnp.maximum(z - 1, 0))

    def across(p, src, step, half):
        part = part_of(p, src, half)
        return pltpu.make_async_remote_copy(
            src_ref=part, dst_ref=part, send_sem=send_y.at[p, src, step - 1],
            recv_sem=recv_y.at[p, src, step - 1],
            device_id={"grp": lax.rem(g + step, n_grp)}, device_id_type=MESH)

    def send_own(p):
        @pl.when(z < n_fs - 1)
        def _():
            right(p, z).start()

        @pl.when(z > 0)
        def _():
            left(p, z).start()

    def pump(p):
        def body(t, _):
            @pl.when(z - t >= 0)
            def _():
                src = jnp.maximum(z - t, 0)
                right(p, src).wait_recv()

                @pl.when(z < n_fs - 1)
                def _():
                    right(p, src).start()

                for step in range(1, n_grp):
                    across(p, src, step, g).start()

            @pl.when(z + t < n_fs)
            def _():
                src = jnp.minimum(z + t, n_fs - 1)
                left(p, src).wait_recv()

                @pl.when(z > 0)
                def _():
                    left(p, src).start()

                for step in range(1, n_grp):
                    across(p, src, step, g).start()

            return 0

        lax.fori_loop(1, n_fs, body, 0)

    def wait_across(p):
        def body(src, _):
            @pl.when(src != z)
            def _():
                for step in range(1, n_grp):
                    across(p, src, step, lax.rem(g + n_grp - step, n_grp)).wait_recv()

            return 0

        lax.fori_loop(0, n_fs, body, 0)

    def drain(p):
        def body(src, _):
            @pl.when((src <= z) & (z < n_fs - 1))
            def _():
                right(p, src).wait_send()

            @pl.when((src >= z) & (z > 0))
            def _():
                left(p, src).wait_send()

            @pl.when(src != z)
            def _():
                for step in range(1, n_grp):
                    across(p, src, step, g).wait_send()

            return 0

        lax.fori_loop(0, n_fs, body, 0)

    def rows_of(c):
        return pl.ds(aligned(c * LEN, LEN), LEN)

    def cols_of(t):
        return pl.ds(aligned(t * E, E), E)

    def gather(i, c, owner, to, slot):
        part = xfull.at[i, rows_of(c), cols_of(owner)]
        return pltpu.make_async_remote_copy(
            src_ref=part, dst_ref=part, send_sem=ag_s.at[i, c, slot], recv_sem=ag_r.at[i, c, owner],
            device_id={"tp": to}, device_id_type=MESH)

    def peer(d):
        return lax.rem(xi + d, n_x) * 2 + par

    def gather_send(i, c):
        for d in range(1, n_x):
            gather(i, c, tp, peer(d), d).start()
        gather(i, c, tp, partner, 0).start()

    def gather_forward(i, c):
        for d in range(1, n_x):
            src = lax.rem(xi + n_x - d, n_x) * 2 + par
            gather(i, c, src, tp, 0).wait_recv()
            gather(i, c, src, partner, n_x + d - 1).start()

    def gather_wait(i, c):
        for j in range(n_x):
            gather(i, c, j * 2 + 1 - par, tp, 0).wait_recv()

    def gather_drain(i, c):
        for slot in range(2 * n_x - 1):
            gather(i, c, tp, partner, slot).wait_send()

    def pair(i, c):
        return pltpu.make_async_remote_copy(
            src_ref=rs1_s.at[i, :, rows_of(c), :], dst_ref=rs1_r.at[i, :, rows_of(c), :],
            send_sem=s1_s.at[i, c], recv_sem=s1_r.at[i, c],
            device_id={"tp": partner}, device_id_type=MESH)

    def cross(i, c, d):
        return pltpu.make_async_remote_copy(
            src_ref=rs2_s.at[i, d - 1, rows_of(c), :], dst_ref=rs2_r.at[i, d - 1, rows_of(c), :],
            send_sem=s2_s.at[i, c, d - 1], recv_sem=s2_r.at[i, c, d - 1],
            device_id={"tp": peer(d)}, device_id_type=MESH)

    def sum_start(i, c):
        for j in range(n_x):
            rs1_s[i, j, rows_of(c), :] = acc[rows_of(c), cols_of(j * 2 + 1 - par)].astype(bf16)
        pair(i, c).start()

    def sum_cross(i, c):
        pair(i, c).wait_recv()
        for d in range(1, n_x):
            j = lax.rem(xi + d, n_x)
            rs2_s[i, d - 1, rows_of(c), :] = (
                acc[rows_of(c), cols_of(j * 2 + par)] + rs1_r[i, j, rows_of(c), :].astype(f32)
            ).astype(bf16)
            cross(i, c, d).start()

    def sum_end(i, c):
        total = acc[rows_of(c), cols_of(tp)] + rs1_r[i, xi, rows_of(c), :].astype(f32)
        for d in range(1, n_x):
            cross(i, c, d).wait_recv()
            total = total + rs2_r[i, d - 1, rows_of(c), :].astype(f32)
        return total

    def each(body):
        def step(c, _):
            body(c)
            return 0

        lax.fori_loop(0, n_ch, step, 0)

    def norm(i, c):
        def body(k, _):
            rows = pl.ds(aligned(c * LEN + k * SUB, SUB), SUB)
            values = xfull[i, rows, :].astype(f32)
            inverse = lax.rsqrt(jnp.sum(values * values, axis=1, keepdims=True) / D + epsilon)
            nbuf[rows, :] = (values * inverse * gfull[pl.ds(i, 1), :]).astype(bf16)
            return 0

        lax.fori_loop(0, LEN // SUB, body, 0)

    def hidden_of(b, c):
        rows = nbuf[rows_of(c), :]
        gate = jnp.dot(rows, gates[b][...], preferred_element_type=f32)
        up = jnp.dot(rows, ups[b][...], preferred_element_type=f32)
        return (gate * jax.nn.sigmoid(gate) * up).astype(bf16)

    barrier = pltpu.get_barrier_semaphore()
    for step in (1, n_fs - 1):
        pl.semaphore_signal(barrier, inc=1, device_id={"fs": lax.rem(z + step, n_fs)}, device_id_type=MESH)
    for step in range(1, n_grp):
        pl.semaphore_signal(barrier, inc=1, device_id={"grp": lax.rem(g + step, n_grp)}, device_id_type=MESH)
    for step in range(1, n_tp):
        pl.semaphore_signal(barrier, inc=1, device_id={"tp": lax.rem(tp + step, n_tp)}, device_id_type=MESH)
    x_copy = pltpu.make_async_copy(x_hbm, xfull.at[0, :, cols_of(tp)], sem_x)
    for p in range(n_p):
        own_copy(p).start()
        if p == LEAD - 1:
            x_copy.start()
    gfull[:, cols_of(tp)] = gains_ref[...]
    pad_ref[pl.ds(0, 32), :] = jnp.zeros((32, C), f32)
    pl.semaphore_wait(barrier, 2 + n_grp - 1 + n_tp - 1)

    def gain_copy(owner, step):
        return pltpu.make_async_remote_copy(
            src_ref=gains_ref, dst_ref=gfull.at[:, cols_of(owner)], send_sem=ga_s.at[step - 1],
            recv_sem=ga_r.at[step - 1], device_id={"tp": lax.rem(tp + step, n_tp)}, device_id_type=MESH)

    for p in range(LEAD):
        own_copy(p).wait()
        send_own(p)
    x_copy.wait()
    each(lambda c: gather_send(0, c))
    for step in range(1, n_tp):
        gain_copy(tp, step).start()
    for p in range(LEAD, n_p):
        own_copy(p).wait()

    queue = []

    def unit(b):
        def run(c):
            hidden = hidden_of(b, c)
            for s in range(n_fs):
                columns = pl.ds(s * downs[b].shape[2], downs[b].shape[2])
                part = jnp.dot(hidden, downs[b][s], preferred_element_type=f32)
                if b == 0:
                    acc[rows_of(c), columns] = part
                else:
                    acc[rows_of(c), columns] += part
        return run

    done = 0
    for p in range(n_p):
        if p + LEAD < n_p:
            send_own(p + LEAD)
        pump(p)
        if p == 0:
            each(lambda c: gather_forward(0, c))
            for step in range(1, n_tp):
                gain_copy(tp, step).wait_recv()
        if p == 1:
            each(lambda c: gather_wait(0, c))
            each(lambda c: norm(0, c))
        if p >= 1 and p - 1 < 3 * n_b:
            wait_across(p - 1)
            if (p - 1) % 3 == 2:
                b = (p - 1) // 3
                each(unit(b))
                if b == n_b - 1:
                    each(lambda c: sum_start(0, c))
    each(lambda c: sum_cross(0, c))

    def close(i, scale):
        def run(c):
            total = sum_end(i, c)
            fresh = xfull[i, rows_of(c), cols_of(tp)].astype(f32) + scale * total
            xfull[i + 1, rows_of(c), cols_of(tp)] = fresh.astype(bf16)
            gather_send(i + 1, c)
        return run

    each(close(0, 0.5))
    for p in range(3 * n_b, n_p):
        wait_across(p)
    each(lambda c: gather_forward(1, c))

    def stat_copy(c, step):
        return pltpu.make_async_remote_copy(
            src_ref=st_s.at[c], dst_ref=st_r.at[c, step - 1], send_sem=ss_s.at[c, step - 1],
            recv_sem=ss_r.at[c, step - 1], device_id={"tp": lax.rem(tp + step, n_tp)}, device_id_type=MESH)

    def conv_front(c):
        gather_wait(1, c)
        norm(1, c)
        rows = nbuf[rows_of(c), :]
        value = jnp.dot(rows, value_w[...], preferred_element_type=f32)
        gating = jnp.dot(rows, glu_w[...], preferred_element_type=f32)
        pad_ref[pl.ds(32, LEN), :] = value * jax.nn.sigmoid(gating)
        total = jnp.zeros((LEN, C), f32)
        for k in range(KERNEL):
            total = total + small_ref[pl.ds(k, 1), :] * pad_ref[pl.ds(33 - KERNEL + k, LEN), :]
        conv_ref[rows_of(c), :] = total
        lanes = lax.broadcasted_iota(jnp.int32, (LEN, 128), 1)
        both = jnp.where(lanes == 0, jnp.sum(total, axis=1, keepdims=True),
                         jnp.sum(total * total, axis=1, keepdims=True))
        st_s[c] = jnp.transpose(both)[0:8, :]
        for step in range(1, n_tp):
            stat_copy(c, step).start()

    each(conv_front)

    def conv_back(c):
        stats = st_s[c]
        for step in range(1, n_tp):
            stat_copy(c, step).wait_recv()
            stats = stats + st_r[c, step - 1]
        stats = jnp.concatenate([stats, jnp.zeros((LEN - 8, LEN), f32)], axis=0)
        turned = jnp.transpose(stats)
        mean = turned[:, 0:1] / (C * n_tp)
        spread = turned[:, 1:2] / (C * n_tp) - mean * mean
        normed = (conv_ref[rows_of(c), :] - mean) * lax.rsqrt(spread + epsilon) * small_ref[
            pl.ds(KERNEL, 1), :] + small_ref[pl.ds(KERNEL + 1, 1), :]
        mixed = (normed * jax.nn.sigmoid(normed)).astype(bf16)
        for s in range(n_fs):
            acc[rows_of(c), pl.ds(s * mix_w.shape[2], mix_w.shape[2])] = jnp.dot(
                mixed, mix_w[s], preferred_element_type=f32)
        sum_start(1, c)

    each(conv_back)
    each(lambda c: sum_cross(1, c))
    each(close(1, 1.0))
    each(lambda c: gather_forward(2, c))

    def second(c):
        gather_wait(2, c)
        norm(2, c)
        start = 0
        for b, w in enumerate(widths):
            hbuf[:, pl.ds(start, w)] = hidden_of(b, c)
            start += w

        @pl.when(c > 0)
        def _():
            sum_cross(2, jnp.maximum(c - 1, 0))

        for s in range(n_fs):
            start = 0
            part = jnp.zeros((LEN, downs[0].shape[2]), f32)
            for b, w in enumerate(widths):
                part = part + jnp.dot(hbuf[:, pl.ds(start, w)], downs[b][s], preferred_element_type=f32)
                start += w
            acc[rows_of(c), pl.ds(s * downs[0].shape[2], downs[0].shape[2])] = part
        sum_start(2, c)

    each(second)
    sum_cross(2, n_ch - 1)

    def last(c):
        total = sum_end(2, c)
        out_ref[rows_of(c), :] = (xfull[2, rows_of(c), cols_of(tp)].astype(f32) + 0.5 * total).astype(bf16)

    each(last)

    for p in range(n_p):
        drain(p)
    for step in range(1, n_tp):
        gain_copy(tp, step).wait_send()

    def leave(c):
        for i in range(3):
            gather_drain(i, c)
            pair(i, c).wait_send()
            for d in range(1, n_x):
                cross(i, c, d).wait_send()
        for step in range(1, n_tp):
            stat_copy(c, step).wait_send()

    each(leave)


def solution(mesh):
    n_grp, n_fs, n_tp = mesh.shape["grp"], mesh.shape["fs"], mesh.shape["tp"]

    def local(
        stream_in, gain_before, gain_mixer, gain_after, w_gate, w_upward, w_down, w_value,
        w_glu_gate, conv_taps, chan_gain, chan_bias, w_mix_out,
    ):
        R, E = stream_in.shape
        DK, F = w_gate.shape
        C = w_value.shape[1]
        E2 = w_down.shape[1]
        D = E * n_tp
        n_x, n_ch = n_tp // 2, R // LEN
        widths = [min(WIDE, F - start) for start in range(0, F, WIDE)]
        cfg = dict(n_grp=n_grp, n_fs=n_fs, n_tp=n_tp, R=R, E=E, DK=DK, F=F, C=C, widths=widths)
        gains = jnp.concatenate(
            [gain_before[None], gain_mixer[None], gain_after[None], jnp.zeros((5, E), bf16)], axis=0
        ).astype(f32)
        small = jnp.concatenate(
            [conv_taps, chan_gain[None], chan_bias[None], jnp.zeros((7, C), bf16)], axis=0
        ).astype(f32)
        n_p = 3 * len(widths) + 3
        dma = pltpu.SemaphoreType.DMA
        scratch = [pltpu.VMEM((D, w), bf16) for w in widths] * 2
        scratch += [pltpu.VMEM((n_fs, w, E2), bf16) for w in widths]
        scratch += [pltpu.VMEM((D, C), bf16)] * 2 + [pltpu.VMEM((n_fs, C, E2), bf16)]
        scratch += [
            pltpu.VMEM((3, R, D), bf16), pltpu.VMEM((R, D), bf16), pltpu.VMEM((R, D), f32),
            pltpu.VMEM((LEN, F), bf16), pltpu.VMEM((32 + LEN, C), f32), pltpu.VMEM((R, C), f32),
            pltpu.VMEM((8, D), f32),
            pltpu.VMEM((3, n_x, R, E), bf16), pltpu.VMEM((3, n_x, R, E), bf16),
            pltpu.VMEM((3, n_x - 1, R, E), bf16), pltpu.VMEM((3, n_x - 1, R, E), bf16),
            pltpu.VMEM((n_ch, 8, LEN), f32), pltpu.VMEM((n_ch, n_tp - 1, 8, LEN), f32),
            dma((n_p,)), dma,
            dma((n_p, n_fs)), dma((n_p, n_fs, n_grp - 1)), dma((n_p, n_fs)), dma((n_p, n_fs)),
            dma((n_p, n_fs, n_grp - 1)),
            dma((n_tp - 1,)), dma((n_tp - 1,)),
            dma((3, n_ch, 2 * n_x - 1)), dma((3, n_ch, n_tp)),
            dma((3, n_ch)), dma((3, n_ch)),
            dma((3, n_ch, n_x - 1)), dma((3, n_ch, n_x - 1)),
            dma((n_ch, n_tp - 1)), dma((n_ch, n_tp - 1)),
        ]
        hbm = pl.BlockSpec(memory_space=pl.ANY)
        vmem = pl.BlockSpec(memory_space=pltpu.VMEM)
        return pl.pallas_call(
            functools.partial(kernel, cfg),
            out_shape=jax.ShapeDtypeStruct((R, E), bf16),
            in_specs=[hbm] * 7 + [vmem] * 2,
            out_specs=vmem,
            scratch_shapes=scratch,
            compiler_params=pltpu.CompilerParams(
                collective_id=0, has_side_effects=True, vmem_limit_bytes=62 * 1024 * 1024),
        )(stream_in, w_gate, w_upward, w_down, w_value, w_glu_gate, w_mix_out, gains, small)

    in_specs = (
        P(("grp", "fs"), "tp"), P("tp"), P("tp"), P("tp"), P("fs", "tp"), P("fs", "tp"),
        P("tp", "fs"), P("fs", "tp"), P("fs", "tp"), P(None, "tp"), P("tp"), P("tp"), P("tp", "fs"),
    )
    return jax.shard_map(
        local, mesh=mesh, in_specs=in_specs, out_specs=P(("grp", "fs"), "tp"), check_vma=False)
```

time: 622 us -> 252 us (0.41)
  waiting for transfers between devices: 525 us -> 0 us
  Pallas kernels: 0 us -> 244 us
  matrix products: 43.9 us -> 0 us
  blocking collectives: 26 us -> 0 us
  between operations: 13.7 us -> 0.01 us
  other arithmetic: 12.7 us -> 2.08 us
    all_gather x9 -> x0, waiting for transfers between devices: 439 us -> none  [the longest x1 108 us: local(): lax.all_gather(w_gate, 'fs', axis=0, tiled=True)]
    pallas_call x0 -> x1, Pallas kernels: none -> 244 us  [local(): pl.pallas_call(functools.partial(kernel, cfg), out_shape=jax.ShapeDtypeSt...]
    reduce_scatter x3 -> x0, waiting for transfers between devices: 81.4 us -> none  [settle(): lax.psum_scatter(partial_term.astype(jnp.bfloat16), 'tp', scatter_dimensi...]
    dot_general x7 -> x0, matrix products: 43.9 us -> none  [the longest x2 22.5 us: feed_forward(): jnp.dot(hidden, whole_down, preferred_element_type=jnp.float32)]
    psum x4 -> x0, blocking collectives: 26 us -> none  [the longest x3 19.9 us: normed_rows(): totals = lax.psum(jnp.sum(values * values, axis=1), 'tp')]
  transfers between devices with their start and end apart: 12 -> 0, of which waited for: 12 -> 0; matrix products, arithmetic and copies ran while one was open for 2% -> 0% of each run, Pallas kernels for 0% -> 0%
where the time goes in v1:
time: 252 us
  Pallas kernels  244 us (97%)
  local copies, waits for them, and re-layouts  5.29 us (2%)
    pallas_call x1, Pallas kernels, local(): pl.pallas_call(functools.partial(kernel, cfg), out_shape=jax.ShapeDtypeSt...  244 us

profile of v1, /device:TPU:0, one launch (start us, length us, event | category | flops | bytes accessed | tf_op | source)
XLA Modules:
  0.0 251.7 jit_solution(2286866343078980828)
XLA Ops:
  0.0 0.1 pad.3.clone
  0.1 0.1 pad.7.clone
  0.2 0.7 broadcast_in_dim.25
  0.8 0.7 broadcast_in_dim.26
  1.5 0.7 broadcast_in_dim.21
  2.2 0.7 broadcast_in_dim.22
  2.8 0.7 broadcast_in_dim.23
  3.5 0.7 maximum_convert_fusion.1.gains_ref
  4.2 1.4 maximum_convert_fusion.small_ref
  5.6 244.3 %shard_map.127 = bf16[384,512]{1,0:T(8,128)(2,1)} custom-call(bf16[384,512]{1,0:T(8,128)(2,1)} %x_hbm.1, bf16[512,1408]{1,0:T(8,128)(2,1)} %gate_hbm.1, bf16[512,1408]{1,0:T(8,128)(2,1)} %up_hbm.1, bf16[1408,512]{1,0:T(8,128)(2,1)} %down_hbm.1, bf16[512,256]{1,0:T(8,128)(2,1)} %value_hbm.1, bf16[512,256]{1,0:T(8,128)(2,1)} %glu_hbm.1, ...), custom_call_target="tpu_custom_call" | custom-call | tf_op jit(solution)/shard_map/pallas_call | solution.py:487
  249.9 1.8 copy.15
  (2 shorter events, 0.0 us)

commit v2 on v1

--- a/solution.py
+++ b/solution.py
@@ -10,8 +10,9 @@
 KERNEL = 31
 LEN = 128
 WIDE = 384
-LEAD = 3
-SUB = 16
+LEAD = 1
+LAG = 1
+SUB = 64
 
 epsilon = 1e-06
 MESH = pl.DeviceIdType.MESH
@@ -117,35 +118,30 @@
         def _():
             left(p, z).start()
 
-    def pump(p):
-        def body(t, _):
-            @pl.when(z - t >= 0)
+    def pump(p, t):
+        @pl.when(z - t >= 0)
+        def _():
+            src = jnp.maximum(z - t, 0)
+            right(p, src).wait_recv()
+
+            @pl.when(z < n_fs - 1)
             def _():
-                src = jnp.maximum(z - t, 0)
-                right(p, src).wait_recv()
-
-                @pl.when(z < n_fs - 1)
-                def _():
-                    right(p, src).start()
-
-                for step in range(1, n_grp):
-                    across(p, src, step, g).start()
-
-            @pl.when(z + t < n_fs)
+                right(p, src).start()
+
+            for step in range(1, n_grp):
+                across(p, src, step, g).start()
+
+        @pl.when(z + t < n_fs)
+        def _():
+            src = jnp.minimum(z + t, n_fs - 1)
+            left(p, src).wait_recv()
+
+            @pl.when(z > 0)
             def _():
-                src = jnp.minimum(z + t, n_fs - 1)
-                left(p, src).wait_recv()
-
-                @pl.when(z > 0)
-                def _():
-                    left(p, src).start()
-
-                for step in range(1, n_grp):
-                    across(p, src, step, g).start()
-
-            return 0
-
-        lax.fori_loop(1, n_fs, body, 0)
+                left(p, src).start()
+
+            for step in range(1, n_grp):
+                across(p, src, step, g).start()
 
     def wait_across(p):
         def body(src, _):
@@ -298,8 +294,6 @@
     for p in range(LEAD, n_p):
         own_copy(p).wait()
 
-    queue = []
-
     def unit(b):
         def run(c):
             hidden = hidden_of(b, c)
@@ -312,27 +306,6 @@
                     acc[rows_of(c), columns] += part
         return run
 
-    done = 0
-    for p in range(n_p):
-        if p + LEAD < n_p:
-            send_own(p + LEAD)
-        pump(p)
-        if p == 0:
-            each(lambda c: gather_forward(0, c))
-            for step in range(1, n_tp):
-                gain_copy(tp, step).wait_recv()
-        if p == 1:
-            each(lambda c: gather_wait(0, c))
-            each(lambda c: norm(0, c))
-        if p >= 1 and p - 1 < 3 * n_b:
-            wait_across(p - 1)
-            if (p - 1) % 3 == 2:
-                b = (p - 1) // 3
-                each(unit(b))
-                if b == n_b - 1:
-                    each(lambda c: sum_start(0, c))
-    each(lambda c: sum_cross(0, c))
-
     def close(i, scale):
         def run(c):
             total = sum_end(i, c)
@@ -341,7 +314,36 @@
             gather_send(i + 1, c)
         return run
 
-    each(close(0, 0.5))
+    after = [
+        lambda: each(lambda c: sum_cross(0, c)),
+        lambda: each(close(0, 0.5)),
+    ]
+    ended = False
+    for k in range(n_p + n_fs - 2):
+        if k + LEAD < n_p:
+            send_own(k + LEAD)
+        for t in range(1, n_fs):
+            if 0 <= k - (t - 1) < n_p:
+                pump(k - (t - 1), t)
+        if ended and after:
+            after.pop(0)()
+        if k == 0:
+            each(lambda c: gather_forward(0, c))
+            for step in range(1, n_tp):
+                gain_copy(tp, step).wait_recv()
+        if k == 1:
+            each(lambda c: gather_wait(0, c))
+            each(lambda c: norm(0, c))
+        q = k - (n_fs - 2) - LAG
+        if 0 <= q < 3 * n_b:
+            wait_across(q)
+            if q % 3 == 2:
+                each(unit(q // 3))
+            if q == 3 * n_b - 1:
+                each(lambda c: sum_start(0, c))
+                ended = True
+    for stage in after:
+        stage()
     for p in range(3 * n_b, n_p):
         wait_across(p)
     each(lambda c: gather_forward(1, c))

time: 252 us -> 243 us (0.964)
  Pallas kernels: 244 us -> 235 us
    pallas_call x1, Pallas kernels: 244 us -> 235 us  [local(): pl.pallas_call(functools.partial(kernel, cfg), out_shape=jax.ShapeDtypeSt...]
where the time goes in v2:
time: 243 us; the launch traced here: 242 us
  Pallas kernels  235 us (97%)
  local copies, waits for them, and re-layouts  5.29 us (2%)
    pallas_call x1, Pallas kernels, local(): pl.pallas_call(functools.partial(kernel, cfg), out_shape=jax.ShapeDtypeSt...  235 us

profile of v2, /device:TPU:0, one launch (start us, length us, event | category | flops | bytes accessed | tf_op | source)
XLA Modules:
  0.0 242.3 jit_solution(9629245124444133055)
XLA Ops:
  0.0 0.1 pad.3.clone
  0.1 0.1 pad.7.clone
  0.2 0.7 broadcast_in_dim.25
  0.8 0.7 broadcast_in_dim.26
  1.5 0.7 broadcast_in_dim.21
  2.2 0.7 broadcast_in_dim.22
  2.8 0.7 broadcast_in_dim.23
  3.5 0.7 maximum_convert_fusion.1.gains_ref
  4.2 1.4 maximum_convert_fusion.small_ref
  5.6 234.9 %shard_map.127 = bf16[384,512]{1,0:T(8,128)(2,1)} custom-call(bf16[384,512]{1,0:T(8,128)(2,1)} %x_hbm.1, bf16[512,1408]{1,0:T(8,128)(2,1)} %gate_hbm.1, bf16[512,1408]{1,0:T(8,128)(2,1)} %up_hbm.1, bf16[1408,512]{1,0:T(8,128)(2,1)} %down_hbm.1, bf16[512,256]{1,0:T(8,128)(2,1)} %value_hbm.1, bf16[512,256]{1,0:T(8,128)(2,1)} %glu_hbm.1, ...), custom_call_target="tpu_custom_call" | custom-call | tf_op jit(solution)/shard_map/pallas_call | solution.py:489
  240.5 1.8 copy.15
  (2 shorter events, 0.0 us)
